TPU v7x, 32 devices: a whole 2x2x4 slice. The times are simulated.
32 devices in a mesh: grp: 2 (over y), ep: 16 (over z, x, core), tp: 1.
Axes of the slice: x: 2, y: 2, z: 4, core: 2. Of those that a mesh axis runs over, the one named last changes fastest.
Arguments:
- tokens: bfloat16 [3072, 2048], P(('grp', 'ep')), parts along dimension 0, may hold values from -6 to 6
- prior_state: float32 [2, 3072, 4096], P(None, ('grp', 'ep'), 'tp'), parts along dimension 1, may hold values from -6 to 6
- mix_gain: float32 [2048], replicated, may hold values from 0.1 to 1.9
- in_weight: bfloat16 [2048, 1024], P(None, 'tp'), may hold values from -0.125 to 0.125
- decay_rate: float32 [64, 64], P('tp'), may hold values from 0.2 to 20
- frequency: float32 [64, 64], P('tp'), may hold values from 0 to 12
- log_step: float32 [64], P('tp'), may hold values from -4.6 to 0
- input_map: float32 [2, 64, 64, 16], P(None, 'tp'), may hold values from -6 to 6
- output_map: float32 [2, 64, 16, 64], P(None, 'tp'), may hold values from -0.5 to 0.5
- skip_gain: float32 [1024], P('tp'), may hold values from -4 to 4
- out_weight: bfloat16 [1024, 2048], P('tp'), may hold values from -0.1875 to 0.1875
- channel_gain: float32 [2048], replicated, may hold values from 0.1 to 1.9
- expert_gate: bfloat16 [16, 2048, 512], P('ep', None, 'tp'), may hold values from -0.125 to 0.125
- expert_up: bfloat16 [16, 2048, 512], P('ep', None, 'tp'), may hold values from -0.125 to 0.125
- expert_down: bfloat16 [16, 512, 2048], P('ep', 'tp'), may hold values from -0.25 to 0.25
- shared_gate: bfloat16 [2048, 512], P(None, 'tp'), may hold values from -0.125 to 0.125
- shared_up: bfloat16 [2048, 512], P(None, 'tp'), may hold values from -0.125 to 0.125
- shared_down: bfloat16 [512, 2048], P('tp'), may hold values from -0.25 to 0.25
- routes: int32 [3072, 6], P(('grp', 'ep')), parts along dimension 0, may hold values from 0 to 15, all different within a row; in each aligned block of 96 rows (0 to 95, 96 to 191, ...) at most 54 rows name the same one
- route_weights: float32 [3072, 6], P(('grp', 'ep')), parts along dimension 0, may hold values from 0.05 to 0.8
Outputs:
- layer_out: bfloat16 [3072, 2048], P(('grp', 'ep'), 'tp'), parts along dimension 0
- new_state: float32 [2, 3072, 4096], P(None, ('grp', 'ep'), 'tp'), parts along dimension 1
There are 2 independent parts, one for each index of `grp`. A program takes and returns all parts, laid end to end along the dimension named above; an argument that names none is the same for every part. Nothing has to cross between parts.
Inputs may be any that keep to these rules, and one draw needn't show every extreme that they name: `routes`: each row names 6 different experts; among the rows of one index of ep no expert is named by more than 54 rows.
All inputs are finite; a program needn't handle non-finite values.
Results may differ from a plain program's by a relative error of at most 0.017.
Values may be sent and summed in bfloat16 or wider, within the bound.
A program may use at most 128 MiB of HBM per device.

v0:
```python
import jax
import jax.numpy as jnp
from jax import lax
from jax.sharding import PartitionSpec as P

norm_eps = 1e-06
highest = lax.Precision.HIGHEST


def root_scale(activations, scale_gain):
    values = activations.astype(jnp.float32)
    factor = lax.rsqrt(jnp.mean(values * values, axis=-1, keepdims=True) + norm_eps)
    return (values * factor * scale_gain).astype(jnp.bfloat16)


def state_update(
    drive_rows, prior_state, decay_rate, frequency, log_step, input_map, output_map, skip_gain
):
    sequences = drive_rows.shape[0]
    groups = decay_rate.shape[0]
    driven = drive_rows.astype(jnp.float32).reshape(sequences, groups, -1)
    step_size = jnp.exp(log_step)[:, None]
    real_rate = -decay_rate
    magnitude = jnp.exp(real_rate * step_size)
    turn_real = magnitude * jnp.cos(frequency * step_size)
    turn_imag = magnitude * jnp.sin(frequency * step_size)
    denominator = real_rate * real_rate + frequency * frequency
    hold_real = ((turn_real - 1.0) * real_rate + turn_imag * frequency) / denominator
    hold_imag = (turn_imag * real_rate - (turn_real - 1.0) * frequency) / denominator
    push_real = jnp.einsum("sgh,gph->sgp", driven, input_map[0], precision=highest)
    push_imag = jnp.einsum("sgh,gph->sgp", driven, input_map[1], precision=highest)
    enter_real = push_real * hold_real - push_imag * hold_imag
    enter_imag = push_real * hold_imag + push_imag * hold_real
    old_real = prior_state[0].reshape(sequences, groups, -1)
    old_imag = prior_state[1].reshape(sequences, groups, -1)
    fresh_real = turn_real * old_real - turn_imag * old_imag + enter_real
    fresh_imag = turn_real * old_imag + turn_imag * old_real + enter_imag
    readout = jnp.einsum("ghp,sgp->sgh", output_map[0], fresh_real, precision=highest)
    readout = readout - jnp.einsum("ghp,sgp->sgh", output_map[1], fresh_imag, precision=highest)
    readout = readout.reshape(sequences, -1) + skip_gain * drive_rows.astype(jnp.float32)
    fresh = jnp.stack([fresh_real.reshape(sequences, -1), fresh_imag.reshape(sequences, -1)])
    return (readout, fresh)


def exchanged_experts(second_normed, routes, route_weights, expert_gate, expert_up, expert_down):
    experts = lax.axis_size("ep")
    seq_rows, top_count = routes.shape
    slot_cap = min(seq_rows, max(2, 3 * seq_rows * top_count // (2 * experts)))
    flat_routes = routes.reshape(-1)
    one_hot = (flat_routes[:, None] == jnp.arange(experts, dtype=jnp.int32)[None, :]).astype(
        jnp.int32
    )
    ranked = jnp.sum((jnp.cumsum(one_hot, axis=0) - one_hot) * one_hot, axis=1)
    slot_index = flat_routes * slot_cap + ranked
    placed = slot_index[:, None] == jnp.arange(experts * slot_cap, dtype=jnp.int32)[None, :]
    placed_rows = jnp.any(placed.reshape(seq_rows, top_count, experts * slot_cap), axis=1).astype(
        jnp.bfloat16
    )
    outgoing = lax.dot_general(
        placed_rows, second_normed, (((0,), (0,)), ((), ())), preferred_element_type=jnp.float32
    ).astype(jnp.bfloat16)
    outgoing = outgoing.reshape(experts, slot_cap, -1)
    arrived = lax.all_to_all(outgoing, "ep", split_axis=0, concat_axis=0, tiled=True)
    sources, count_items, full_width = arrived.shape
    expert_rows = arrived.reshape(sources * count_items, full_width)
    gate_val = jnp.dot(expert_rows, expert_gate[0], preferred_element_type=jnp.float32)
    up_val = jnp.dot(expert_rows, expert_up[0], preferred_element_type=jnp.float32)
    hidden = (jax.nn.silu(gate_val) * up_val).astype(jnp.bfloat16)
    piece = jnp.dot(hidden, expert_down[0], preferred_element_type=jnp.float32)
    summed = lax.psum_scatter(
        piece.reshape(sources, count_items, full_width).astype(jnp.bfloat16),
        "tp",
        scatter_dimension=2,
        tiled=True,
    )
    returned = lax.all_to_all(summed, "ep", split_axis=0, concat_axis=0, tiled=True)
    flat_back = returned.reshape(experts * slot_cap, -1)
    picked = (
        jnp.take(flat_back, slot_index, axis=0).reshape(seq_rows, top_count, -1).astype(jnp.float32)
    )
    routed = jnp.einsum("sk,skd->sd", route_weights, picked)
    return routed


def gathered_experts(second_normed, routes, route_weights, expert_gate, expert_up, expert_down):
    all_routes = lax.all_gather(routes, "ep", axis=0, tiled=True)
    all_weights = lax.all_gather(route_weights, "ep", axis=0, tiled=True)
    here = all_routes == lax.axis_index("ep")
    weight = jnp.sum(jnp.where(here, all_weights, 0.0), axis=1)
    rows = lax.all_gather(second_normed, "ep", axis=0, tiled=True)
    gate_val = jnp.dot(rows, expert_gate[0], preferred_element_type=jnp.float32)
    up_val = jnp.dot(rows, expert_up[0], preferred_element_type=jnp.float32)
    hidden = (jax.nn.silu(gate_val) * up_val).astype(jnp.bfloat16)
    piece = jnp.dot(hidden, expert_down[0], preferred_element_type=jnp.float32)
    summed = lax.psum_scatter(piece.astype(jnp.bfloat16), "tp", scatter_dimension=1, tiled=True)
    weighted = (weight[:, None] * summed.astype(jnp.float32)).astype(jnp.bfloat16)
    return lax.psum_scatter(weighted, "ep", scatter_dimension=0, tiled=True).astype(jnp.float32)


def body(
    tokens,
    prior_state,
    mix_gain,
    in_weight,
    decay_rate,
    frequency,
    log_step,
    input_map,
    output_map,
    skip_gain,
    out_weight,
    channel_gain,
    expert_gate,
    expert_up,
    expert_down,
    shared_gate,
    shared_up,
    shared_down,
    routes,
    route_weights,
):
    normed = root_scale(tokens, mix_gain)
    drive_rows = jnp.dot(normed, in_weight, preferred_element_type=jnp.float32).astype(jnp.bfloat16)
    readout, new_state = state_update(
        drive_rows, prior_state, decay_rate, frequency, log_step, input_map, output_map, skip_gain
    )
    activated = jax.nn.gelu(readout).astype(jnp.bfloat16)
    partial_value = jnp.dot(activated, out_weight, preferred_element_type=jnp.float32)
    mixer_out = lax.psum(partial_value.astype(jnp.bfloat16), "tp").astype(jnp.float32)
    middle = (tokens.astype(jnp.float32) + mixer_out).astype(jnp.bfloat16)
    second_normed = root_scale(middle, channel_gain)
    shared_gval = jnp.dot(second_normed, shared_gate, preferred_element_type=jnp.float32)
    shared_uval = jnp.dot(second_normed, shared_up, preferred_element_type=jnp.float32)
    shared_hidden = (jax.nn.silu(shared_gval) * shared_uval).astype(jnp.bfloat16)
    shared_piece = jnp.dot(shared_hidden, shared_down, preferred_element_type=jnp.float32)
    shared_out = lax.psum_scatter(
        shared_piece.astype(jnp.bfloat16), "tp", scatter_dimension=1, tiled=True
    ).astype(jnp.float32)
    experts = lax.axis_size("ep")
    half_cols = second_normed.shape[1] // lax.axis_size("tp")
    if experts <= 16:
        routed = gathered_experts(
            second_normed, routes, route_weights, expert_gate, expert_up, expert_down
        )
    else:
        routed = exchanged_experts(
            second_normed, routes, route_weights, expert_gate, expert_up, expert_down
        )
    own_middle = lax.dynamic_slice_in_dim(middle, lax.axis_index("tp") * half_cols, half_cols, 1)
    layer_out = (own_middle.astype(jnp.float32) + routed + shared_out).astype(jnp.bfloat16)
    return (layer_out, new_state)


def solution(mesh):
    in_specs = (
        P(("grp", "ep"), None),
        P(None, ("grp", "ep"), "tp"),
        P(),
        P(None, "tp"),
        P("tp", None),
        P("tp", None),
        P("tp"),
        P(None, "tp", None, None),
        P(None, "tp", None, None),
        P("tp"),
        P("tp", None),
        P(),
        P("ep", None, "tp"),
        P("ep", None, "tp"),
        P("ep", "tp", None),
        P(None, "tp"),
        P(None, "tp"),
        P("tp", None),
        P(("grp", "ep"), None),
        P(("grp", "ep"), None),
    )
    out_specs = (P(("grp", "ep"), "tp"), P(None, ("grp", "ep"), "tp"))
    return jax.shard_map(body, mesh=mesh, in_specs=in_specs, out_specs=out_specs, check_vma=False)
```

profile of v0, /device:TPU:0, one launch (start us, length us, event | category | flops | bytes accessed | tf_op | source)
XLA Modules:
  0.0 219.6 jit_solution(10515037456347401280)
XLA Ops:
  7.2 0.0 copy-start
  7.2 0.0 all-gather.4.cloned.1.call-start
  7.2 0.8 exp.14
  8.0 1.2 fusion.13
  9.2 3.2 %convolution_convert_fusion.3 = bf16[96,1024]{1,0:T(8,128)(2,1)S(1)} fusion(bf16[2048,1024]{1,0:T(8,128)(2,1)} %param.23, bf16[96,2048]{1,0:T(8,128)(2,1)} %param.20, f32[2048]{0:T(1024)} %param.22, f32[96]{0:T(128)S(1)} %add_rsqrt_fusion.1), kind=kOutput, calls=%fused_computation.23 | convolution fusion | flops 403537920 | bytes 4792704 | tf_op jit(solution)/shard_map/dot_general | solution.py:123
  12.4 0.2 copy.37
  12.6 3.8 %fusion.58 = (f32[1,96,4096]{2,1,0:T(8,128)}, f32[1,96,4096]{2,1,0:T(8,128)}) fusion(f32[2,96,4096]{2,1,0:T(8,128)} %param.21), kind=kLoop, calls=%fused_computation.79 | loop fusion | bytes 6291456 | tf_op jit(solution)/shard_map/slice | solution.py:34
  16.4 2.8 %copy.35 = f32[1,96,4096]{1,2,0:T(8,128)} copy(f32[1,96,4096]{2,1,0:T(8,128)} %get-tuple-element.4) | data formatting | bytes 3145728 | tf_op jit(solution)/shard_map/slice | solution.py:34
  19.2 2.8 %copy.36 = f32[1,96,4096]{1,2,0:T(8,128)} copy(f32[1,96,4096]{2,1,0:T(8,128)} %get-tuple-element.5) | data formatting | bytes 3145728 | tf_op jit(solution)/shard_map/slice | solution.py:35
  22.0 3.0 %fusion.23 = f32[64,96,64]{1,2,0:T(8,128)S(1)} fusion(bf16[96,64,16]{0,2,1:T(8,128)(2,1)S(1)} %bitcast.56, f32[2,64,64,16]{2,3,1,0:T(8,128)} %param.27), kind=kOutput, calls=%fused_computation.37 | convolution fusion | flops 75497472 | bytes 2293760 | tf_op jit(solution)/shard_map/sgh,gph->sgp/dot_general | solution.py:30
  25.1 0.0 copy-done.8
  25.1 0.0 copy-done.9
  25.1 0.2 cosine_multiply_fusion
  25.3 0.0 copy-done.3
  25.3 0.0 copy-start.7
  25.3 5.7 %bitcast_add_fusion = (f32[96,64,64]{0,2,1:T(8,128)S(1)}, f32[96,64,64]{0,2,1:T(8,128)S(1)}) fusion(f32[64,96,64]{1,2,0:T(8,128)S(1)} %fusion.23, f32[96,64,64]{0,2,1:T(8,128)S(1)} %bitcast.54, f32[96,64,64]{0,2,1:T(8,128)} %bitcast.55, f32[64,64]{1,0:T(8,128)S(1)} %get-tuple-element.8, f32[64,64]{1,0:T(8,128)S(1)} %get-tuple-element.7, ...), kind=kOutput, calls=%fused_computation.18 | convolution fusion | flops 81002496 | bytes 9175040 | tf_op jit(solution)/shard_map/sgh,gph->sgp/dot_general | solution.py:31
  31.0 0.0 copy-start.1
  31.0 0.0 copy-start.2
  31.1 0.0 copy-done.7
  31.1 1.9 fusion.19
  33.0 0.0 copy-start.13
  33.0 1.9 convolution_subtract_fusion
  34.9 0.0 copy-done.1
  34.9 0.0 copy-done.2
  34.9 0.9 copy.38
  35.9 0.0 copy-done.6
  35.9 0.0 copy-done.13
  35.9 0.0 copy-start.12
  35.9 3.3 %multiply_reduce_fusion = (f32[96]{0:T(128)S(1)}, f32[96,2048]{1,0:T(8,128)S(1)}) fusion(bf16[1024,2048]{1,0:T(8,128)(2,1)} %param.30, f32[96,1024]{1,0:T(8,128)} %copy.38, bf16[96,1024]{1,0:T(8,128)(2,1)S(1)} %convolution_convert_fusion.3, f32[1024]{0:T(1024)S(1)} %copy-done.13, bf16[96,2048]{1,0:T(8,128)(2,1)S(1)} %copy-done.6), kind=kOutput, calls=%fused_computation.30 | convolution fusion | flops 405405600 | bytes 5968256 | tf_op jit(solution)/shard_map/dot_general | solution.py:128
  39.2 0.0 copy-done.10
  39.2 0.9 multiply_convert_fusion.1
  40.1 0.0 all-gather.4.cloned.1.call-update
  40.2 0.0 reduce-scatter.2.cloned.1.call-start
  40.2 23.8 %all-gather = s32[16,96,6]{1,2,0:T(8,128)S(1)} all-gather(s32[1,96,6]{1,2,0:T(8,128)S(1)} %bitcast.59), channel_id=1, replica_groups=mesh['grp'=2,'ep'=16,'tp'=1] {'ep'}, dimensions={0}, use_global_device_ids=true | all-gather | bytes 39168 | tf_op jit(solution)/shard_map/all_gather | solution.py:86
  64.0 18.2 %all-gather.1 = f32[16,96,6]{1,2,0:T(8,128)S(1)} all-gather(f32[1,96,6]{1,2,0:T(8,128)S(1)} %bitcast.60), channel_id=1, replica_groups=mesh['grp'=2,'ep'=16,'tp'=1] {'ep'}, dimensions={0}, use_global_device_ids=true | all-gather | bytes 39168 | tf_op jit(solution)/shard_map/all_gather | solution.py:87
  82.2 0.1 reshape.45
  82.3 22.4 %all-gather.4.cloned.1.call-done = bf16[1536,2048]{1,0:T(8,128)(2,1)} async-done(((bf16[96,2048]{1,0:T(8,128)(2,1)}), bf16[1536,2048]{1,0:T(8,128)(2,1)}) %all-gather.4.cloned.1.call-update) | async-done | bytes 6291472 | tf_op jit(solution)/shard_map/all_gather | solution.py:90
  104.7 8.5 %fusion.10 = f32[1536,512]{1,0:T(8,128)} fusion(bf16[1536,2048]{1,0:T(8,128)(2,1)} %all-gather.4.cloned.1.call-done, bf16[1,2048,512]{2,1,0:T(8,128)(2,1)} %param.32), kind=kOutput, calls=%fused_computation.16 | convolution fusion | flops 3221225472 | bytes 11534336 | tf_op jit(solution)/shard_map/dot_general | solution.py:91
  113.2 0.0 copy-done
  113.2 11.8 %multiply_convert_fusion = bf16[1536,2048]{1,0:T(8,128)(2,1)} fusion(f32[1536]{0:T(1024)S(1)} %reshape.45, bf16[1,512,2048]{2,1,0:T(8,128)(2,1)S(1)} %copy-done, bf16[1536,2048]{1,0:T(8,128)(2,1)} %all-gather.4.cloned.1.call-done, f32[1536,512]{1,0:T(8,128)} %fusion.10, bf16[1,2048,512]{2,1,0:T(8,128)(2,1)} %param.33), kind=kOutput, calls=%fused_computation | convolution fusion | flops 6459752448 | bytes 19929088 | tf_op jit(solution)/shard_map/dot_general | solution.py:94
  125.0 0.0 reduce-scatter.2.cloned.1.call-update
  125.0 2.8 %copy.39 = f32[1,96,4096]{2,1,0:T(8,128)} copy(f32[1,96,4096]{1,2,0:T(8,128)} %bitcast.53) | data formatting | bytes 3145728 | tf_op jit(solution)/shard_map/stack;reshape | solution.py:41
  127.8 2.9 %copy.40 = f32[1,96,4096]{2,1,0:T(8,128)} copy(f32[1,96,4096]{1,2,0:T(8,128)} %bitcast.52) | data formatting | bytes 3145728 | tf_op jit(solution)/shard_map/stack;reshape | solution.py:41
  130.7 2.4 %fusion.59 = f32[96,512]{1,0:T(8,128)S(1)} fusion(bf16[96,2048]{1,0:T(8,128)(2,1)S(1)} %copy-done.5, bf16[2048,512]{1,0:T(8,128)(2,1)} %param.35), kind=kOutput, calls=%fused_computation.80 | convolution fusion | flops 201326592 | bytes 2686976 | tf_op jit(solution)/shard_map/dot_general | solution.py:132
  133.1 0.0 copy-done.4
  133.1 3.4 %pad_maximum_fusion = f32[2,96,4096]{2,1,0:T(8,128)} fusion(f32[1,96,4096]{2,1,0:T(8,128)} %copy.40, f32[1,96,4096]{2,1,0:T(8,128)S(1)} %copy-done.4), kind=kLoop, calls=%fused_computation.3 | loop fusion | flops 786432 | bytes 6291456 | tf_op jit(solution)/shard_map/stack | solution.py:41
  136.5 72.4 %reduce-scatter.2.cloned.1.call-done = bf16[96,2048]{1,0:T(8,128)(2,1)} async-done(((bf16[1536,2048]{1,0:T(8,128)(2,1)}), bf16[96,2048]{1,0:T(8,128)(2,1)}) %reduce-scatter.2.cloned.1.call-update) | async-done | bytes 393232 | tf_op jit(solution)/shard_map/reduce_scatter | solution.py:97
  208.9 3.9 %fusion.3 = bf16[96,2048]{1,0:T(8,128)(2,1)} fusion(bf16[512,2048]{1,0:T(8,128)(2,1)} %param.37, bf16[96,2048]{1,0:T(8,128)(2,1)S(1)} %copy-done.5, bf16[2048,512]{1,0:T(8,128)(2,1)} %param.36, f32[96,2048]{1,0:T(8,128)S(1)} %get-tuple-element.11, bf16[96,2048]{1,0:T(8,128)(2,1)} %reduce-scatter.2.cloned.1.call-done, f32[96,512]{1,0:T(8,128)S(1)} %fusion.59), kind=kOutput, calls=%fused_computation.8 | convolution fusion | flops 404127744 | bytes 6356992 | tf_op jit(solution)/shard_map/dot_general | solution.py:135
  (14 shorter events, 0.1 us)
Async XLA Ops:
  7.2 106.0 %copy-start = (bf16[1,512,2048]{2,1,0:T(8,128)(2,1)S(1)}, bf16[1,512,2048]{2,1,0:T(8,128)(2,1)}, u32[]{:S(2)}) copy-start(bf16[1,512,2048]{2,1,0:T(8,128)(2,1)} %param.34) | copy-start | bytes 6291460
  7.2 97.5 %all-gather.4.cloned.1.call-start = ((), (), s32[]{:S(2)}) async-start(), calls=%async_computation.1 | async-start | bytes 6684672 | tf_op jit(solution)/shard_map/all_gather | solution.py:90
  22.0 3.0 %copy-start.8 = (f32[64,64]{1,0:T(8,128)S(1)}, f32[64,64]{1,0:T(8,128)}, u32[]{:S(2)}) copy-start(f32[64,64]{1,0:T(8,128)} %param.25) | copy-start | bytes 49156
  22.0 3.0 %copy-start.9 = (f32[64,64]{1,0:T(8,128)S(1)}, f32[64,64]{1,0:T(8,128)}, u32[]{:S(2)}) copy-start(f32[64,64]{1,0:T(8,128)} %param.24) | copy-start | bytes 49156
  22.0 3.3 %copy-start.3 = (f32[1,96,4096]{1,2,0:T(8,128)S(1)}, f32[1,96,4096]{1,2,0:T(8,128)}, u32[]{:S(2)}) copy-start(f32[1,96,4096]{1,2,0:T(8,128)} %copy.35) | copy-start | bytes 4718596
  25.3 5.7 %copy-start.7 = (f32[2,64,16,64]{3,2,1,0:T(8,128)S(1)}, f32[2,64,16,64]{3,2,1,0:T(8,128)}, u32[]{:S(2)}) copy-start(f32[2,64,16,64]{3,2,1,0:T(8,128)} %param.28) | copy-start | bytes 1572868
  31.0 3.9 %copy-start.1 = (f32[96,64,64]{0,2,1:T(8,128)}, f32[96,64,64]{0,2,1:T(8,128)S(1)}, u32[]{:S(2)}) copy-start(f32[96,64,64]{0,2,1:T(8,128)S(1)} %get-tuple-element.2) | copy-start | bytes 4718596
  31.0 3.9 %copy-start.2 = (f32[96,64,64]{0,2,1:T(8,128)}, f32[96,64,64]{0,2,1:T(8,128)S(1)}, u32[]{:S(2)}) copy-start(f32[96,64,64]{0,2,1:T(8,128)S(1)} %get-tuple-element.3) | copy-start | bytes 4718596
  33.0 2.9 %copy-start.6 = (bf16[96,2048]{1,0:T(8,128)(2,1)S(1)}, bf16[96,2048]{1,0:T(8,128)(2,1)}, u32[]{:S(2)}) copy-start(bf16[96,2048]{1,0:T(8,128)(2,1)} %param.20) | copy-start | bytes 1179652
  33.0 2.9 %copy-start.13 = (f32[1024]{0:T(1024)S(1)}, f32[1024]{0:T(1024)}, u32[]{:S(2)}) copy-start(f32[1024]{0:T(1024)} %param.29) | copy-start | bytes 12292
  35.9 3.4 %copy-start.10 = (f32[2048]{0:T(1024)S(1)}, f32[2048]{0:T(1024)}, u32[]{:S(2)}) copy-start(f32[2048]{0:T(1024)} %param.31) | copy-start | bytes 24580
  35.9 4.3 %copy-start.11 = (s32[96,6]{0,1:T(8,128)S(1)}, s32[96,6]{0,1:T(8,128)}, u32[]{:S(2)}) copy-start(s32[96,6]{0,1:T(8,128)} %param.38) | copy-start | bytes 6916
  35.9 28.1 %copy-start.12 = (f32[96,6]{0,1:T(8,128)S(1)}, f32[96,6]{0,1:T(8,128)}, u32[]{:S(2)}) copy-start(f32[96,6]{0,1:T(8,128)} %param.39) | copy-start | bytes 6916
  40.2 168.7 %reduce-scatter.2.cloned.1.call-start = ((), (), s32[]{:S(2)}) async-start(), calls=%async_computation.2 | async-start | bytes 6684672 | tf_op jit(solution)/shard_map/reduce_scatter | solution.py:97
  127.8 2.9 %copy-start.5 = (bf16[96,2048]{1,0:T(8,128)(2,1)S(1)}, bf16[96,2048]{1,0:T(8,128)(2,1)}, u32[]{:S(2)}) copy-start(bf16[96,2048]{1,0:T(8,128)(2,1)} %multiply_convert_fusion.1) | copy-start | bytes 1179652
  130.7 2.4 %copy-start.4 = (f32[1,96,4096]{2,1,0:T(8,128)S(1)}, f32[1,96,4096]{2,1,0:T(8,128)}, u32[]{:S(2)}) copy-start(f32[1,96,4096]{2,1,0:T(8,128)} %copy.39) | copy-start | bytes 4718596
Sparse Core Ops, SparseCore 0:
  40.3 64.3 all-gather.3
  125.1 83.7 reduce-scatter.1
where the time goes:
time: 220 us
  waiting for transfers between devices  94.8 us (43%)
  matrix products  45.6 us (21%)
  blocking collectives  42 us (19%)
  local copies, waits for them, and re-layouts  17.2 us (8%)
  between operations  14.2 us (6%)
  other arithmetic  5.75 us (3%)
    reduce_scatter x1, waiting for transfers between devices, gathered_experts(): lax.psum_scatter(weighted, 'ep', scatter_dimension=0, tiled=True)  72.4 us
    all_gather x1, blocking collectives, gathered_experts(): all_routes = lax.all_gather(routes, 'ep', axis=0, tiled=True)  23.8 us
    all_gather x1, waiting for transfers between devices, gathered_experts(): rows = lax.all_gather(second_normed, 'ep', axis=0, tiled=True)  22.4 us
    all_gather x1, blocking collectives, gathered_experts(): all_weights = lax.all_gather(route_weights, 'ep', axis=0, tiled=True)  18.2 us
    dot_general x1, matrix products, gathered_experts(): piece = jnp.dot(hidden, expert_down[0], preferred_element_type=jnp.float32)  11.8 us
    dot_general x1, matrix products, gathered_experts(): gate_val = jnp.dot(rows, expert_gate[0], preferred_element_type=jnp.float32)  8.51 us
    slice x2, local copies, waits for them, and re-layouts, state_update(): old_real = prior_state[0].reshape(sequences, groups, -1)  6.61 us
    another operation x2, local copies, waits for them, and re-layouts, state_update(): jnp.stack([fresh_real.reshape(sequences, -1), fresh_imag.reshape(sequence...  5.71 us
  transfers between devices with their start and end apart: 2, of which 2 were waited for; matrix products, arithmetic and copies ran while one was open for 5% of the time, Pallas kernels for 0%

commit v1 on v0

--- a/solution.py
+++ b/solution.py
@@ -84,7 +84,12 @@
 
 def gathered_experts(second_normed, routes, route_weights, expert_gate, expert_up, expert_down):
     all_routes = lax.all_gather(routes, "ep", axis=0, tiled=True)
-    all_weights = lax.all_gather(route_weights, "ep", axis=0, tiled=True)
+    ring = [route_weights]
+    for hop in range(15):
+        ring.append(lax.ppermute(ring[-1], "ep", [(dev, (dev + 1) % 16) for dev in range(16)]))
+    all_weights = jnp.roll(
+        jnp.concatenate(ring[::-1], axis=0), (lax.axis_index("ep") + 1) * ring[0].shape[0], axis=0
+    )
     here = all_routes == lax.axis_index("ep")
     weight = jnp.sum(jnp.where(here, all_weights, 0.0), axis=1)
     rows = lax.all_gather(second_normed, "ep", axis=0, tiled=True)

time: 220 us -> 256 us (1.16)
  waiting for transfers between devices: 94.8 us -> 153 us
  blocking collectives: 42 us -> 18.1 us
    ppermute x0 -> x15, waiting for transfers between devices: none -> 81.6 us  [gathered_experts(): lax.ppermute(ring[-1], 'ep', [(dev, (dev + 1) % 16) for dev in range(16)])]
    all_gather x1, waiting for transfers between devices: 22.4 us -> 0.02 us  [gathered_experts(): rows = lax.all_gather(second_normed, 'ep', axis=0, tiled=True)]
    all_gather x1 -> x0, blocking collectives: 18.2 us -> none  [gathered_experts(): all_weights = lax.all_gather(route_weights, 'ep', axis=0, tiled=True)]
    all_gather x1, blocking collectives: 23.8 us -> 18.1 us  [gathered_experts(): all_routes = lax.all_gather(routes, 'ep', axis=0, tiled=True)]
  transfers between devices with their start and end apart: 2 -> 17, of which waited for: 2 -> 15; matrix products, arithmetic and copies ran while one was open for 5% -> 5% of each run, Pallas kernels for 0% -> 0%
where the time goes in v1:
time: 256 us; the launch traced here: 255 us
  waiting for transfers between devices  153 us (60%)
  matrix products  45.6 us (18%)
  blocking collectives  18.1 us (7%)
  local copies, waits for them, and re-layouts  17.3 us (7%)
  between operations  14.3 us (6%)
  other arithmetic  5.84 us (2%)
    ppermute x15, waiting for transfers between devices, gathered_experts(): lax.ppermute(ring[-1], 'ep', [(dev, (dev + 1) % 16) for dev in range(16)])  81.6 us
    reduce_scatter x1, waiting for transfers between devices, gathered_experts(): lax.psum_scatter(weighted, 'ep', scatter_dimension=0, tiled=True)  71.8 us
    all_gather x1, blocking collectives, gathered_experts(): all_routes = lax.all_gather(routes, 'ep', axis=0, tiled=True)  18.1 us
    dot_general x1, matrix products, gathered_experts(): piece = jnp.dot(hidden, expert_down[0], preferred_element_type=jnp.float32)  11.8 us
    dot_general x1, matrix products, gathered_experts(): gate_val = jnp.dot(rows, expert_gate[0], preferred_element_type=jnp.float32)  8.52 us
    slice x2, local copies, waits for them, and re-layouts, state_update(): old_real = prior_state[0].reshape(sequences, groups, -1)  6.59 us
    another operation x2, local copies, waits for them, and re-layouts, state_update(): jnp.stack([fresh_real.reshape(sequences, -1), fresh_imag.reshape(sequence...  5.73 us
    dot_general x1, matrix products, state_update(): jnp.einsum('sgh,gph->sgp', driven, input_map[1], precision=highest)  5.71 us
  transfers between devices with their start and end apart: 17, of which 15 were waited for; matrix products, arithmetic and copies ran while one was open for 5% of the time, Pallas kernels for 0%

profile of v1, /device:TPU:0, one launch (start us, length us, event | category | flops | bytes accessed | tf_op | source)
XLA Modules:
  0.0 255.4 jit_solution(12569279599424782163)
XLA Ops:
  7.2 0.0 all-gather.3.cloned.1.call-start
  7.2 0.8 exp.14
  8.0 1.2 fusion.15
  9.2 3.2 %convolution_convert_fusion.3 = bf16[96,1024]{1,0:T(8,128)(2,1)S(1)} fusion(bf16[2048,1024]{1,0:T(8,128)(2,1)} %param.23, bf16[96,2048]{1,0:T(8,128)(2,1)} %param.20, f32[2048]{0:T(1024)} %param.22, f32[96]{0:T(128)S(1)} %add_rsqrt_fusion.1), kind=kOutput, calls=%fused_computation.23 | convolution fusion | flops 403537920 | bytes 4792704 | tf_op jit(solution)/shard_map/dot_general | solution.py:128
  12.4 0.2 copy.52
  12.6 3.8 %fusion.60 = (f32[1,96,4096]{2,1,0:T(8,128)}, f32[1,96,4096]{2,1,0:T(8,128)}) fusion(f32[2,96,4096]{2,1,0:T(8,128)} %param.21), kind=kLoop, calls=%fused_computation.80 | loop fusion | bytes 6291456 | tf_op jit(solution)/shard_map/slice | solution.py:34
  16.4 2.8 %copy.50 = f32[1,96,4096]{1,2,0:T(8,128)} copy(f32[1,96,4096]{2,1,0:T(8,128)} %get-tuple-element.4) | data formatting | bytes 3145728 | tf_op jit(solution)/shard_map/slice | solution.py:34
  19.2 2.8 %copy.51 = f32[1,96,4096]{1,2,0:T(8,128)} copy(f32[1,96,4096]{2,1,0:T(8,128)} %get-tuple-element.5) | data formatting | bytes 3145728 | tf_op jit(solution)/shard_map/slice | solution.py:35
  22.0 3.0 %fusion.25 = f32[64,96,64]{1,2,0:T(8,128)S(1)} fusion(bf16[96,64,16]{0,2,1:T(8,128)(2,1)S(1)} %bitcast.59, f32[2,64,64,16]{2,3,1,0:T(8,128)} %param.27), kind=kOutput, calls=%fused_computation.37 | convolution fusion | flops 75497472 | bytes 2293760 | tf_op jit(solution)/shard_map/sgh,gph->sgp/dot_general | solution.py:30
  25.0 0.2 cosine_multiply_fusion
  25.3 5.7 %bitcast_add_fusion = (f32[96,64,64]{0,2,1:T(8,128)S(1)}, f32[96,64,64]{0,2,1:T(8,128)S(1)}) fusion(f32[64,96,64]{1,2,0:T(8,128)S(1)} %fusion.25, f32[96,64,64]{0,2,1:T(8,128)S(1)} %bitcast.57, f32[96,64,64]{0,2,1:T(8,128)} %bitcast.58, f32[64,64]{1,0:T(8,128)S(1)} %get-tuple-element.8, f32[64,64]{1,0:T(8,128)S(1)} %get-tuple-element.7, ...), kind=kOutput, calls=%fused_computation.18 | convolution fusion | flops 81002496 | bytes 9175040 | tf_op jit(solution)/shard_map/sgh,gph->sgp/dot_general | solution.py:31
  31.0 1.9 fusion.21
  33.0 1.9 convolution_subtract_fusion
  34.9 0.9 copy.53
  35.9 3.3 %multiply_reduce_fusion = (f32[96]{0:T(128)S(1)}, f32[96,2048]{1,0:T(8,128)S(1)}) fusion(bf16[1024,2048]{1,0:T(8,128)(2,1)} %param.30, f32[96,1024]{1,0:T(8,128)} %copy.53, bf16[96,1024]{1,0:T(8,128)(2,1)S(1)} %convolution_convert_fusion.3, f32[1024]{0:T(1024)S(1)} %copy-done.13, bf16[96,2048]{1,0:T(8,128)(2,1)S(1)} %copy-done.6), kind=kOutput, calls=%fused_computation.30 | convolution fusion | flops 405405600 | bytes 5968256 | tf_op jit(solution)/shard_map/dot_general | solution.py:133
  39.2 0.9 multiply_convert_fusion.1
  40.1 0.0 all-gather.3.cloned.1.call-update
  40.1 0.0 reduce-scatter.2.cloned.1.call-start
  40.2 0.5 collective-permute-start
  40.7 6.2 %collective-permute-done = f32[96,6]{0,1:T(8,128)S(1)} collective-permute-done((f32[96,6]{0,1:T(8,128)S(1)}, f32[96,6]{0,1:T(8,128)S(1)}, u32[]{:S(2)}, u32[]{:S(2)}) %collective-permute-start) | collective-permute-done | bytes 2336 | tf_op jit(solution)/shard_map/ppermute | solution.py:89
  47.0 5.7 %collective-permute-done.1 = f32[96,6]{0,1:T(8,128)S(1)} collective-permute-done((f32[96,6]{0,1:T(8,128)S(1)}, f32[96,6]{0,1:T(8,128)S(1)}, u32[]{:S(2)}, u32[]{:S(2)}) %collective-permute-start.1) | collective-permute-done | bytes 2336 | tf_op jit(solution)/shard_map/ppermute | solution.py:89
  52.7 5.9 %collective-permute-done.2 = f32[96,6]{0,1:T(8,128)S(1)} collective-permute-done((f32[96,6]{0,1:T(8,128)S(1)}, f32[96,6]{0,1:T(8,128)S(1)}, u32[]{:S(2)}, u32[]{:S(2)}) %collective-permute-start.2) | collective-permute-done | bytes 2336 | tf_op jit(solution)/shard_map/ppermute | solution.py:89
  58.6 5.9 %collective-permute-done.3 = f32[96,6]{0,1:T(8,128)S(1)} collective-permute-done((f32[96,6]{0,1:T(8,128)S(1)}, f32[96,6]{0,1:T(8,128)S(1)}, u32[]{:S(2)}, u32[]{:S(2)}) %collective-permute-start.3) | collective-permute-done | bytes 2336 | tf_op jit(solution)/shard_map/ppermute | solution.py:89
  64.5 5.7 %collective-permute-done.4 = f32[96,6]{0,1:T(8,128)S(1)} collective-permute-done((f32[96,6]{0,1:T(8,128)S(1)}, f32[96,6]{0,1:T(8,128)S(1)}, u32[]{:S(2)}, u32[]{:S(2)}) %collective-permute-start.4) | collective-permute-done | bytes 2336 | tf_op jit(solution)/shard_map/ppermute | solution.py:89
  70.3 5.8 %collective-permute-done.5 = f32[96,6]{0,1:T(8,128)S(1)} collective-permute-done((f32[96,6]{0,1:T(8,128)S(1)}, f32[96,6]{0,1:T(8,128)S(1)}, u32[]{:S(2)}, u32[]{:S(2)}) %collective-permute-start.5) | collective-permute-done | bytes 2336 | tf_op jit(solution)/shard_map/ppermute | solution.py:89
  76.1 5.9 %collective-permute-done.6 = f32[96,6]{0,1:T(8,128)S(1)} collective-permute-done((f32[96,6]{0,1:T(8,128)S(1)}, f32[96,6]{0,1:T(8,128)S(1)}, u32[]{:S(2)}, u32[]{:S(2)}) %collective-permute-start.6) | collective-permute-done | bytes 2336 | tf_op jit(solution)/shard_map/ppermute | solution.py:89
  82.0 5.9 %collective-permute-done.7 = f32[96,6]{0,1:T(8,128)S(1)} collective-permute-done((f32[96,6]{0,1:T(8,128)S(1)}, f32[96,6]{0,1:T(8,128)S(1)}, u32[]{:S(2)}, u32[]{:S(2)}) %collective-permute-start.7) | collective-permute-done | bytes 2336 | tf_op jit(solution)/shard_map/ppermute | solution.py:89
  88.0 5.8 %collective-permute-done.8 = f32[96,6]{0,1:T(8,128)S(1)} collective-permute-done((f32[96,6]{0,1:T(8,128)S(1)}, f32[96,6]{0,1:T(8,128)S(1)}, u32[]{:S(2)}, u32[]{:S(2)}) %collective-permute-start.8) | collective-permute-done | bytes 2336 | tf_op jit(solution)/shard_map/ppermute | solution.py:89
  93.7 6.0 %collective-permute-done.9 = f32[96,6]{0,1:T(8,128)S(1)} collective-permute-done((f32[96,6]{0,1:T(8,128)S(1)}, f32[96,6]{0,1:T(8,128)S(1)}, u32[]{:S(2)}, u32[]{:S(2)}) %collective-permute-start.9) | collective-permute-done | bytes 2336 | tf_op jit(solution)/shard_map/ppermute | solution.py:89
  99.8 5.7 %collective-permute-done.10 = f32[96,6]{0,1:T(8,128)S(1)} collective-permute-done((f32[96,6]{0,1:T(8,128)S(1)}, f32[96,6]{0,1:T(8,128)S(1)}, u32[]{:S(2)}, u32[]{:S(2)}) %collective-permute-start.10) | collective-permute-done | bytes 2336 | tf_op jit(solution)/shard_map/ppermute | solution.py:89
  105.5 5.7 %collective-permute-done.11 = f32[96,6]{0,1:T(8,128)S(1)} collective-permute-done((f32[96,6]{0,1:T(8,128)S(1)}, f32[96,6]{0,1:T(8,128)S(1)}, u32[]{:S(2)}, u32[]{:S(2)}) %collective-permute-start.11) | collective-permute-done | bytes 2336 | tf_op jit(solution)/shard_map/ppermute | solution.py:89
  111.3 5.7 %collective-permute-done.12 = f32[96,6]{0,1:T(8,128)S(1)} collective-permute-done((f32[96,6]{0,1:T(8,128)S(1)}, f32[96,6]{0,1:T(8,128)S(1)}, u32[]{:S(2)}, u32[]{:S(2)}) %collective-permute-start.12) | collective-permute-done | bytes 2336 | tf_op jit(solution)/shard_map/ppermute | solution.py:89
  117.0 18.1 %all-gather = s32[16,96,6]{1,2,0:T(8,128)S(1)} all-gather(s32[1,96,6]{1,2,0:T(8,128)S(1)} %bitcast.62), channel_id=1, replica_groups=mesh['grp'=2,'ep'=16,'tp'=1] {'ep'}, dimensions={0}, use_global_device_ids=true | all-gather | bytes 39168 | tf_op jit(solution)/shard_map/all_gather | solution.py:86
  135.1 0.2 collective-permute-start.14
  135.3 0.1 reshape.40
  135.5 5.4 %collective-permute-done.14 = f32[96,6]{0,1:T(8,128)S(1)} collective-permute-done((f32[96,6]{0,1:T(8,128)S(1)}, f32[96,6]{0,1:T(8,128)S(1)}, u32[]{:S(2)}, u32[]{:S(2)}) %collective-permute-start.14) | collective-permute-done | bytes 2336 | tf_op jit(solution)/shard_map/ppermute | solution.py:89
  140.9 0.1 concatenate.6
  141.0 0.1 select_reduce_fusion
  141.1 0.0 all-gather.3.cloned.1.call-done
  141.1 8.5 %fusion.12 = f32[1536,512]{1,0:T(8,128)} fusion(bf16[1536,2048]{1,0:T(8,128)(2,1)} %all-gather.3.cloned.1.call-done, bf16[1,2048,512]{2,1,0:T(8,128)(2,1)} %param.32), kind=kOutput, calls=%fused_computation.16 | convolution fusion | flops 3221225472 | bytes 11534336 | tf_op jit(solution)/shard_map/dot_general | solution.py:96
  149.6 11.8 %multiply_convert_fusion = bf16[1536,2048]{1,0:T(8,128)(2,1)} fusion(f32[1536]{0:T(1024)S(1)} %select_reduce_fusion, bf16[1,512,2048]{2,1,0:T(8,128)(2,1)S(1)} %copy-done, bf16[1536,2048]{1,0:T(8,128)(2,1)} %all-gather.3.cloned.1.call-done, f32[1536,512]{1,0:T(8,128)} %fusion.12, bf16[1,2048,512]{2,1,0:T(8,128)(2,1)} %param.33), kind=kOutput, calls=%fused_computation | convolution fusion | flops 6459752448 | bytes 19929088 | tf_op jit(solution)/shard_map/dot_general | solution.py:99
  161.4 0.0 reduce-scatter.2.cloned.1.call-update
  161.4 2.8 %copy.55 = f32[1,96,4096]{2,1,0:T(8,128)} copy(f32[1,96,4096]{1,2,0:T(8,128)} %bitcast.56) | data formatting | bytes 3145728 | tf_op jit(solution)/shard_map/stack;reshape | solution.py:41
  164.2 3.0 %copy.56 = f32[1,96,4096]{2,1,0:T(8,128)} copy(f32[1,96,4096]{1,2,0:T(8,128)} %bitcast.55) | data formatting | bytes 3145728 | tf_op jit(solution)/shard_map/stack;reshape | solution.py:41
  167.2 2.3 fusion.61
  169.5 3.4 %pad_maximum_fusion = f32[2,96,4096]{2,1,0:T(8,128)} fusion(f32[1,96,4096]{2,1,0:T(8,128)} %copy.56, f32[1,96,4096]{2,1,0:T(8,128)S(1)} %copy-done.4), kind=kLoop, calls=%fused_computation.3 | loop fusion | flops 786432 | bytes 6291456 | tf_op jit(solution)/shard_map/stack | solution.py:41
  172.9 71.8 %reduce-scatter.2.cloned.1.call-done = bf16[96,2048]{1,0:T(8,128)(2,1)} async-done(((bf16[1536,2048]{1,0:T(8,128)(2,1)}), bf16[96,2048]{1,0:T(8,128)(2,1)}) %reduce-scatter.2.cloned.1.call-update) | async-done | bytes 393232 | tf_op jit(solution)/shard_map/reduce_scatter | solution.py:102
  244.7 3.9 %fusion.3 = bf16[96,2048]{1,0:T(8,128)(2,1)} fusion(bf16[512,2048]{1,0:T(8,128)(2,1)} %param.37, bf16[96,2048]{1,0:T(8,128)(2,1)S(1)} %copy-done.5, bf16[2048,512]{1,0:T(8,128)(2,1)} %param.36, f32[96,2048]{1,0:T(8,128)S(1)} %get-tuple-element.11, bf16[96,2048]{1,0:T(8,128)(2,1)} %reduce-scatter.2.cloned.1.call-done, f32[96,512]{1,0:T(8,128)S(1)} %fusion.61), kind=kOutput, calls=%fused_computation.8 | convolution fusion | flops 404127744 | bytes 6356992 | tf_op jit(solution)/shard_map/dot_general | solution.py:140
  (45 shorter events, 0.1 us)
Async XLA Ops:
  7.2 142.5 %copy-start = (bf16[1,512,2048]{2,1,0:T(8,128)(2,1)S(1)}, bf16[1,512,2048]{2,1,0:T(8,128)(2,1)}, u32[]{:S(2)}) copy-start(bf16[1,512,2048]{2,1,0:T(8,128)(2,1)} %param.34) | copy-start | bytes 6291460
  7.2 133.9 %all-gather.3.cloned.1.call-start = ((), (), s32[]{:S(2)}) async-start(), calls=%async_computation.1 | async-start | bytes 6684672 | tf_op jit(solution)/shard_map/all_gather | solution.py:95
  22.0 3.0 %copy-start.8 = (f32[64,64]{1,0:T(8,128)S(1)}, f32[64,64]{1,0:T(8,128)}, u32[]{:S(2)}) copy-start(f32[64,64]{1,0:T(8,128)} %param.25) | copy-start | bytes 49156
  22.0 3.0 %copy-start.9 = (f32[64,64]{1,0:T(8,128)S(1)}, f32[64,64]{1,0:T(8,128)}, u32[]{:S(2)}) copy-start(f32[64,64]{1,0:T(8,128)} %param.24) | copy-start | bytes 49156
  22.0 3.3 %copy-start.3 = (f32[1,96,4096]{1,2,0:T(8,128)S(1)}, f32[1,96,4096]{1,2,0:T(8,128)}, u32[]{:S(2)}) copy-start(f32[1,96,4096]{1,2,0:T(8,128)} %copy.50) | copy-start | bytes 4718596
  25.3 5.8 %copy-start.7 = (f32[2,64,16,64]{3,2,1,0:T(8,128)S(1)}, f32[2,64,16,64]{3,2,1,0:T(8,128)}, u32[]{:S(2)}) copy-start(f32[2,64,16,64]{3,2,1,0:T(8,128)} %param.28) | copy-start | bytes 1572868
  31.0 3.9 %copy-start.1 = (f32[96,64,64]{0,2,1:T(8,128)}, f32[96,64,64]{0,2,1:T(8,128)S(1)}, u32[]{:S(2)}) copy-start(f32[96,64,64]{0,2,1:T(8,128)S(1)} %get-tuple-element.2) | copy-start | bytes 4718596
  31.0 3.9 %copy-start.2 = (f32[96,64,64]{0,2,1:T(8,128)}, f32[96,64,64]{0,2,1:T(8,128)S(1)}, u32[]{:S(2)}) copy-start(f32[96,64,64]{0,2,1:T(8,128)S(1)} %get-tuple-element.3) | copy-start | bytes 4718596
  32.9 2.9 %copy-start.6 = (bf16[96,2048]{1,0:T(8,128)(2,1)S(1)}, bf16[96,2048]{1,0:T(8,128)(2,1)}, u32[]{:S(2)}) copy-start(bf16[96,2048]{1,0:T(8,128)(2,1)} %param.20) | copy-start | bytes 1179652
  32.9 2.9 %copy-start.13 = (f32[1024]{0:T(1024)S(1)}, f32[1024]{0:T(1024)}, u32[]{:S(2)}) copy-start(f32[1024]{0:T(1024)} %param.29) | copy-start | bytes 12292
  35.8 3.4 %copy-start.11 = (f32[2048]{0:T(1024)S(1)}, f32[2048]{0:T(1024)}, u32[]{:S(2)}) copy-start(f32[2048]{0:T(1024)} %param.31) | copy-start | bytes 24580
  35.8 4.3 %copy-start.10 = (f32[96,6]{0,1:T(8,128)S(1)}, f32[96,6]{0,1:T(8,128)}, u32[]{:S(2)}) copy-start(f32[96,6]{0,1:T(8,128)} %param.39) | copy-start | bytes 6916
  35.8 81.1 %copy-start.12 = (s32[96,6]{0,1:T(8,128)S(1)}, s32[96,6]{0,1:T(8,128)}, u32[]{:S(2)}) copy-start(s32[96,6]{0,1:T(8,128)} %param.38) | copy-start | bytes 6916
  40.1 204.6 %reduce-scatter.2.cloned.1.call-start = ((), (), s32[]{:S(2)}) async-start(), calls=%async_computation.2 | async-start | bytes 6684672 | tf_op jit(solution)/shard_map/reduce_scatter | solution.py:102
  40.2 6.8 %collective-permute-start = (f32[96,6]{0,1:T(8,128)S(1)}, f32[96,6]{0,1:T(8,128)S(1)}, u32[]{:S(2)}, u32[]{:S(2)}) collective-permute-start(f32[96,6]{0,1:T(8,128)S(1)} %copy-done.10), channel_id=1, source_target_pairs={{0,1},{1,2},{2,3},{3,4},{4,5},{5,6},{6,7},{7,8},{8,9},{9,10},{10,1... | collective-permute-start | bytes 6920 | tf_op jit(solution)/shard_map/ppermute | solution.py:89
  47.0 5.7 %collective-permute-start.1 = (f32[96,6]{0,1:T(8,128)S(1)}, f32[96,6]{0,1:T(8,128)S(1)}, u32[]{:S(2)}, u32[]{:S(2)}) collective-permute-start(f32[96,6]{0,1:T(8,128)S(1)} %collective-permute-done), channel_id=1, source_target_pairs={{0,1},{1,2},{2,3},{3,4},{4,5},{5,6},{6,7},{7,8},{8,9},{9,10},{10,1... | collective-permute-start | bytes 6920 | tf_op jit(solution)/shard_map/ppermute | solution.py:89
  52.7 5.9 %collective-permute-start.2 = (f32[96,6]{0,1:T(8,128)S(1)}, f32[96,6]{0,1:T(8,128)S(1)}, u32[]{:S(2)}, u32[]{:S(2)}) collective-permute-start(f32[96,6]{0,1:T(8,128)S(1)} %collective-permute-done.1), channel_id=1, source_target_pairs={{0,1},{1,2},{2,3},{3,4},{4,5},{5,6},{6,7},{7,8},{8,9},{9,10},{10,1... | collective-permute-start | bytes 6920 | tf_op jit(solution)/shard_map/ppermute | solution.py:89
  58.6 5.9 %collective-permute-start.3 = (f32[96,6]{0,1:T(8,128)S(1)}, f32[96,6]{0,1:T(8,128)S(1)}, u32[]{:S(2)}, u32[]{:S(2)}) collective-permute-start(f32[96,6]{0,1:T(8,128)S(1)} %collective-permute-done.2), channel_id=1, source_target_pairs={{0,1},{1,2},{2,3},{3,4},{4,5},{5,6},{6,7},{7,8},{8,9},{9,10},{10,1... | collective-permute-start | bytes 6920 | tf_op jit(solution)/shard_map/ppermute | solution.py:89
  64.5 5.7 %collective-permute-start.4 = (f32[96,6]{0,1:T(8,128)S(1)}, f32[96,6]{0,1:T(8,128)S(1)}, u32[]{:S(2)}, u32[]{:S(2)}) collective-permute-start(f32[96,6]{0,1:T(8,128)S(1)} %collective-permute-done.3), channel_id=1, source_target_pairs={{0,1},{1,2},{2,3},{3,4},{4,5},{5,6},{6,7},{7,8},{8,9},{9,10},{10,1... | collective-permute-start | bytes 6920 | tf_op jit(solution)/shard_map/ppermute | solution.py:89
  70.2 5.8 %collective-permute-start.5 = (f32[96,6]{0,1:T(8,128)S(1)}, f32[96,6]{0,1:T(8,128)S(1)}, u32[]{:S(2)}, u32[]{:S(2)}) collective-permute-start(f32[96,6]{0,1:T(8,128)S(1)} %collective-permute-done.4), channel_id=1, source_target_pairs={{0,1},{1,2},{2,3},{3,4},{4,5},{5,6},{6,7},{7,8},{8,9},{9,10},{10,1... | collective-permute-start | bytes 6920 | tf_op jit(solution)/shard_map/ppermute | solution.py:89
  76.1 6.0 %collective-permute-start.6 = (f32[96,6]{0,1:T(8,128)S(1)}, f32[96,6]{0,1:T(8,128)S(1)}, u32[]{:S(2)}, u32[]{:S(2)}) collective-permute-start(f32[96,6]{0,1:T(8,128)S(1)} %collective-permute-done.5), channel_id=1, source_target_pairs={{0,1},{1,2},{2,3},{3,4},{4,5},{5,6},{6,7},{7,8},{8,9},{9,10},{10,1... | collective-permute-start | bytes 6920 | tf_op jit(solution)/shard_map/ppermute | solution.py:89
  82.0 6.0 %collective-permute-start.7 = (f32[96,6]{0,1:T(8,128)S(1)}, f32[96,6]{0,1:T(8,128)S(1)}, u32[]{:S(2)}, u32[]{:S(2)}) collective-permute-start(f32[96,6]{0,1:T(8,128)S(1)} %collective-permute-done.6), channel_id=1, source_target_pairs={{0,1},{1,2},{2,3},{3,4},{4,5},{5,6},{6,7},{7,8},{8,9},{9,10},{10,1... | collective-permute-start | bytes 6920 | tf_op jit(solution)/shard_map/ppermute | solution.py:89
  88.0 5.8 %collective-permute-start.8 = (f32[96,6]{0,1:T(8,128)S(1)}, f32[96,6]{0,1:T(8,128)S(1)}, u32[]{:S(2)}, u32[]{:S(2)}) collective-permute-start(f32[96,6]{0,1:T(8,128)S(1)} %collective-permute-done.7), channel_id=1, source_target_pairs={{0,1},{1,2},{2,3},{3,4},{4,5},{5,6},{6,7},{7,8},{8,9},{9,10},{10,1... | collective-permute-start | bytes 6920 | tf_op jit(solution)/shard_map/ppermute | solution.py:89
  93.7 6.0 %collective-permute-start.9 = (f32[96,6]{0,1:T(8,128)S(1)}, f32[96,6]{0,1:T(8,128)S(1)}, u32[]{:S(2)}, u32[]{:S(2)}) collective-permute-start(f32[96,6]{0,1:T(8,128)S(1)} %collective-permute-done.8), channel_id=1, source_target_pairs={{0,1},{1,2},{2,3},{3,4},{4,5},{5,6},{6,7},{7,8},{8,9},{9,10},{10,1... | collective-permute-start | bytes 6920 | tf_op jit(solution)/shard_map/ppermute | solution.py:89
  99.8 5.7 %collective-permute-start.10 = (f32[96,6]{0,1:T(8,128)S(1)}, f32[96,6]{0,1:T(8,128)S(1)}, u32[]{:S(2)}, u32[]{:S(2)}) collective-permute-start(f32[96,6]{0,1:T(8,128)S(1)} %collective-permute-done.9), channel_id=1, source_target_pairs={{0,1},{1,2},{2,3},{3,4},{4,5},{5,6},{6,7},{7,8},{8,9},{9,10},{10,1... | collective-permute-start | bytes 6920 | tf_op jit(solution)/shard_map/ppermute | solution.py:89
  105.5 5.7 %collective-permute-start.11 = (f32[96,6]{0,1:T(8,128)S(1)}, f32[96,6]{0,1:T(8,128)S(1)}, u32[]{:S(2)}, u32[]{:S(2)}) collective-permute-start(f32[96,6]{0,1:T(8,128)S(1)} %collective-permute-done.10), channel_id=1, source_target_pairs={{0,1},{1,2},{2,3},{3,4},{4,5},{5,6},{6,7},{7,8},{8,9},{9,10},{10,1... | collective-permute-start | bytes 6920 | tf_op jit(solution)/shard_map/ppermute | solution.py:89
  111.2 5.7 %collective-permute-start.12 = (f32[96,6]{0,1:T(8,128)S(1)}, f32[96,6]{0,1:T(8,128)S(1)}, u32[]{:S(2)}, u32[]{:S(2)}) collective-permute-start(f32[96,6]{0,1:T(8,128)S(1)} %collective-permute-done.11), channel_id=1, source_target_pairs={{0,1},{1,2},{2,3},{3,4},{4,5},{5,6},{6,7},{7,8},{8,9},{9,10},{10,1... | collective-permute-start | bytes 6920 | tf_op jit(solution)/shard_map/ppermute | solution.py:89
  117.0 18.2 %collective-permute-start.13 = (f32[96,6]{0,1:T(8,128)S(1)}, f32[96,6]{0,1:T(8,128)S(1)}, u32[]{:S(2)}, u32[]{:S(2)}) collective-permute-start(f32[96,6]{0,1:T(8,128)S(1)} %collective-permute-done.12), channel_id=1, source_target_pairs={{0,1},{1,2},{2,3},{3,4},{4,5},{5,6},{6,7},{7,8},{8,9},{9,10},{10,1... | collective-permute-start | bytes 6920 | tf_op jit(solution)/shard_map/ppermute | solution.py:89
  135.1 5.7 %collective-permute-start.14 = (f32[96,6]{0,1:T(8,128)S(1)}, f32[96,6]{0,1:T(8,128)S(1)}, u32[]{:S(2)}, u32[]{:S(2)}) collective-permute-start(f32[96,6]{0,1:T(8,128)S(1)} %collective-permute-done.13), channel_id=1, source_target_pairs={{0,1},{1,2},{2,3},{3,4},{4,5},{5,6},{6,7},{7,8},{8,9},{9,10},{10,1... | collective-permute-start | bytes 6920 | tf_op jit(solution)/shard_map/ppermute | solution.py:89
  164.2 3.0 %copy-start.5 = (bf16[96,2048]{1,0:T(8,128)(2,1)S(1)}, bf16[96,2048]{1,0:T(8,128)(2,1)}, u32[]{:S(2)}) copy-start(bf16[96,2048]{1,0:T(8,128)(2,1)} %multiply_convert_fusion.1) | copy-start | bytes 1179652
  167.2 2.3 copy-start.4
Sparse Core Ops, SparseCore 0:
  40.2 64.3 all-gather.2
  161.5 83.0 reduce-scatter.1
